TPU v7x, 32 devices: a whole 2x2x4 slice. The times are simulated.
32 devices in a mesh: grp: 2 (over y), fs: 4 (over z), tp: 4 (over x, core).
Axes of the slice: x: 2, y: 2, z: 4, core: 2. Of those that a mesh axis runs over, the one named last changes fastest.
Arguments:
- residual_in: bfloat16 [4096, 2048], P(('grp', 'fs', 'tp')), parts along dimension 0, may hold values from -6 to 6
- hidden_first: bfloat16 [4096, 5632], P(('grp', 'fs', 'tp')), parts along dimension 0, may hold values from -6 to 6
- down_weight: bfloat16 [5632, 2048], P('tp', 'fs'), may hold values from -0.078125 to 0.078125
- mixer_out: bfloat16 [4096, 2048], P(('grp', 'fs', 'tp')), parts along dimension 0, may hold values from -6 to 6
- norm_gain: float32 [2, 2048], replicated, may hold values from 0.1 to 1.9
- norm_shift: float32 [2, 2048], replicated, may hold values from -1.5 to 1.5
- gate_weight: bfloat16 [2048, 5632], P('fs', 'tp'), may hold values from -0.125 to 0.125
- up_weight: bfloat16 [2048, 5632], P('fs', 'tp'), may hold values from -0.125 to 0.125
Outputs:
- mixed_state: bfloat16 [4096, 2048], P(('grp', 'fs', 'tp')), parts along dimension 0
- hidden_second: bfloat16 [4096, 5632], P(('grp', 'fs'), 'tp'), parts along dimension 0
There are 2 independent parts, one for each index of `grp`. A program takes and returns all parts, laid end to end along the dimension named above; an argument that names none is the same for every part. Nothing has to cross between parts.
All inputs are finite; a program needn't handle non-finite values.
Results may differ from a plain program's by a relative error of at most 0.012.
Values may be sent and summed in bfloat16 or wider, within the bound.
A program may use at most 64 MiB of HBM per device.

v0:
```python
import jax
import jax.numpy as jnp
from jax import lax
from jax.sharding import PartitionSpec as P


def layer_norm(values, gain, shift):
    center = values - jnp.mean(values, axis=-1, keepdims=True)
    variance = jnp.mean(center * center, axis=-1, keepdims=True)
    return center * lax.rsqrt(variance + 1e-05) * gain + shift


def on_device(
    residual_in, hidden_first, down_weight, mixer_out, norm_gain, norm_shift, gate_weight, up_weight
):
    spread = lax.all_to_all(hidden_first, "tp", split_axis=1, concat_axis=0, tiled=True)
    down_full = lax.all_gather(down_weight, "fs", axis=1, tiled=True)
    branch = lax.psum_scatter(
        jnp.dot(spread, down_full, preferred_element_type=jnp.float32).astype(jnp.bfloat16),
        "tp",
        scatter_dimension=0,
        tiled=True,
    ).astype(jnp.float32)
    first = layer_norm(
        jnp.sqrt(2.0) * residual_in.astype(jnp.float32) + 0.5 * branch, norm_gain[0], norm_shift[0]
    )
    mixed_state = layer_norm(
        jnp.sqrt(2.0) * first + mixer_out.astype(jnp.float32), norm_gain[1], norm_shift[1]
    ).astype(jnp.bfloat16)
    gathered = lax.all_gather(mixed_state, "tp", axis=0, tiled=True)
    width = gate_weight.shape[1]
    joined = jnp.concatenate([gate_weight, up_weight], axis=1)
    both = jnp.dot(
        gathered,
        lax.all_gather(joined, "fs", axis=0, tiled=True),
        preferred_element_type=jnp.float32,
    )
    gate = both[:, :width]
    up = both[:, width:]
    hidden_second = (jax.nn.silu(gate) * up).astype(jnp.bfloat16)
    return (mixed_state, hidden_second)


def solution(mesh):
    in_specs = (
        P(("grp", "fs", "tp"), None),
        P(("grp", "fs", "tp"), None),
        P("tp", "fs"),
        P(("grp", "fs", "tp"), None),
        P(),
        P(),
        P("fs", "tp"),
        P("fs", "tp"),
    )
    out_specs = (P(("grp", "fs", "tp"), None), P(("grp", "fs"), "tp"))
    return jax.shard_map(
        on_device, mesh=mesh, in_specs=in_specs, out_specs=out_specs, check_vma=False
    )
```

profile of v0, /device:TPU:0, one launch (start us, length us, event | category | flops | bytes accessed | tf_op | source)
XLA Modules:
  0.0 405.8 jit_solution(10597806756419352990)
XLA Ops:
  7.2 0.0 all-gather.4.cloned.1.call-start
  7.2 0.7 all-gather.4.cloned.1.call-update
  7.9 0.0 reduce-scatter.2.cloned.1.call-start
  7.9 1.8 copy.10
  9.8 22.7 %all_to_all.19 = bf16[128,4,1408]{0,2,1:T(8,128)(2,1)S(1)} all-to-all(bf16[128,4,1408]{0,2,1:T(8,128)(2,1)S(1)} %bitcast.12), channel_id=1, replica_groups=mesh['grp'=2,'fs'=4,'tp'=4] {'tp'}, dimensions={1} | all-to-all | bytes 2883584 | tf_op jit(solution)/shard_map/all_to_all | solution.py:16
  32.5 0.8 copy.11
  33.3 85.7 %all-gather.4.cloned.1.call-done = bf16[1408,2048]{1,0:T(8,128)(2,1)} async-done(((bf16[1408,512]{1,0:T(8,128)(2,1)}), bf16[1408,2048]{1,0:T(8,128)(2,1)}) %all-gather.4.cloned.1.call-update) | async-done | bytes 5767184 | tf_op jit(solution)/shard_map/all_gather | solution.py:17
  119.0 0.0 copy-start.3
  119.0 0.0 copy-start.4
  119.0 0.0 copy-start
  119.0 7.2 %convolution_convert_fusion = bf16[512,2048]{1,0:T(8,128)(2,1)} fusion(bf16[512,1408]{1,0:T(8,128)(2,1)S(1)} %bitcast.13, bf16[1408,2048]{1,0:T(8,128)(2,1)} %all-gather.4.cloned.1.call-done), kind=kOutput, calls=%fused_computation | convolution fusion | flops 2953838592 | bytes 9306112 | tf_op jit(solution)/shard_map/dot_general | solution.py:19
  126.2 0.0 reduce-scatter.2.cloned.1.call-update
  126.3 0.0 all-gather.6.cloned.1.call-start
  126.3 0.0 copy-done.3
  126.3 0.0 copy-done.4
  126.4 29.5 %reduce-scatter.2.cloned.1.call-done = bf16[128,2048]{1,0:T(8,128)(2,1)} async-done(((bf16[512,2048]{1,0:T(8,128)(2,1)}), bf16[128,2048]{1,0:T(8,128)(2,1)}) %reduce-scatter.2.cloned.1.call-update) | async-done | bytes 524304 | tf_op jit(solution)/shard_map/reduce_scatter | solution.py:18
  155.9 0.0 copy-done
  155.9 1.3 fusion.1
  157.2 1.4 multiply_reduce_fusion.1
  158.6 0.0 copy-start.1
  158.6 0.0 copy-start.2
  158.6 1.9 fusion.2
  160.5 0.3 multiply_reduce_fusion
  160.8 1.1 add_convert_fusion
  161.8 0.0 all-gather.6.cloned.1.call-update
  161.9 0.0 all-gather.8.cloned.1.call-start
  161.9 0.0 copy-done.1
  161.9 0.0 copy-done.2
  161.9 1.9 pad_maximum_fusion
  163.8 0.0 all-gather.8.cloned.1.call-update
  163.8 20.8 %all-gather.6.cloned.1.call-done = bf16[512,2048]{1,0:T(8,128)(2,1)} async-done(((bf16[128,2048]{1,0:T(8,128)(2,1)}), bf16[512,2048]{1,0:T(8,128)(2,1)}) %all-gather.6.cloned.1.call-update) | async-done | bytes 2097168 | tf_op jit(solution)/shard_map/all_gather | solution.py:30
  184.6 202.5 %all-gather.8.cloned.1.call-done = bf16[2048,2816]{1,0:T(8,128)(2,1)} async-done(((bf16[512,2816]{1,0:T(8,128)(2,1)}), bf16[2048,2816]{1,0:T(8,128)(2,1)}) %all-gather.8.cloned.1.call-update) | async-done | bytes 11534352 | tf_op jit(solution)/shard_map/all_gather | solution.py:35
  387.1 10.2 %fusion.5 = f32[512,2816]{1,0:T(8,128)S(1)} fusion(bf16[512,2048]{1,0:T(8,128)(2,1)} %all-gather.6.cloned.1.call-done, bf16[2048,2816]{1,0:T(8,128)(2,1)} %all-gather.8.cloned.1.call-done), kind=kOutput, calls=%fused_computation.17 | convolution fusion | flops 5905580032 | bytes 19398656 | tf_op jit(solution)/shard_map/dot_general | solution.py:33
  397.3 2.0 fusion
  (6 shorter events, 0.1 us)
Async XLA Ops:
  7.2 111.8 %all-gather.4.cloned.1.call-start = ((), (), s32[]{:S(2)}) async-start(), calls=%async_computation.2 | async-start | bytes 7208960 | tf_op jit(solution)/shard_map/all_gather | solution.py:17
  7.9 148.0 %reduce-scatter.2.cloned.1.call-start = ((), (), s32[]{:S(2)}) async-start(), calls=%async_computation.3 | async-start | bytes 2621440 | tf_op jit(solution)/shard_map/reduce_scatter | solution.py:18
  119.0 7.3 %copy-start.3 = (f32[2,2048]{1,0:T(2,128)S(1)}, f32[2,2048]{1,0:T(2,128)}, u32[]{:S(2)}) copy-start(f32[2,2048]{1,0:T(2,128)} %param.12) | copy-start | bytes 49156
  119.0 7.4 %copy-start.4 = (f32[2,2048]{1,0:T(2,128)S(1)}, f32[2,2048]{1,0:T(2,128)}, u32[]{:S(2)}) copy-start(f32[2,2048]{1,0:T(2,128)} %param.13) | copy-start | bytes 49156
  119.0 36.9 %copy-start = (bf16[128,2048]{1,0:T(8,128)(2,1)S(1)}, bf16[128,2048]{1,0:T(8,128)(2,1)}, u32[]{:S(2)}) copy-start(bf16[128,2048]{1,0:T(8,128)(2,1)} %param.8) | copy-start | bytes 1572868
  126.3 58.3 %all-gather.6.cloned.1.call-start = ((), (), s32[]{:S(2)}) async-start(), calls=%async_computation.4 | async-start | bytes 2621440 | tf_op jit(solution)/shard_map/all_gather | solution.py:30
  158.6 3.3 copy-start.1
  158.6 3.3 copy-start.2
  161.9 225.2 %all-gather.8.cloned.1.call-start = ((), (), s32[]{:S(2)}) async-start(), calls=%async_computation.5 | async-start | bytes 14417920 | tf_op jit(solution)/shard_map/all_gather | solution.py:35
Sparse Core Ops, SparseCore 0:
  9.5 109.3 all-gather.3
  126.4 29.4 reduce-scatter.1
  162.0 22.5 all-gather.5
  186.0 201.0 all-gather.7
where the time goes:
time: 406 us
  waiting for transfers between devices  339 us (83%)
  blocking collectives  22.7 us (6%)
  matrix products  17.4 us (4%)
  between operations  13.9 us (3%)
  other arithmetic  9.78 us (2%)
    all_gather x1, waiting for transfers between devices, on_device(): lax.all_gather(joined, 'fs', axis=0, tiled=True)  202 us
    all_gather x1, waiting for transfers between devices, on_device(): down_full = lax.all_gather(down_weight, 'fs', axis=1, tiled=True)  85.7 us
    reduce_scatter x1, waiting for transfers between devices, on_device(): lax.psum_scatter(jnp.dot(spread, down_full, preferred_element_type=jnp.fl...  29.5 us
    all_to_all x1, blocking collectives, on_device(): lax.all_to_all(hidden_first, 'tp', split_axis=1, concat_axis=0, tiled=True)  22.7 us
    all_gather x1, waiting for transfers between devices, on_device(): gathered = lax.all_gather(mixed_state, 'tp', axis=0, tiled=True)  20.8 us
    dot_general x1, matrix products, on_device(): jnp.dot(gathered, lax.all_gather(joined, 'fs', axis=0, tiled=True), prefe...  10.2 us
  transfers between devices with their start and end apart: 4, of which 4 were waited for; matrix products, arithmetic and copies ran while one was open for 1% of the time, Pallas kernels for 0%

commit v1 on v0

--- a/solution.py
+++ b/solution.py
@@ -32,7 +32,9 @@
     joined = jnp.concatenate([gate_weight, up_weight], axis=1)
     both = jnp.dot(
         gathered,
-        lax.all_gather(joined, "fs", axis=0, tiled=True),
+        jnp.concatenate(
+            lax.all_to_all(jnp.stack([joined] * lax.axis_size("fs")), "fs", 0, 0), axis=0
+        ),
         preferred_element_type=jnp.float32,
     )
     gate = both[:, :width]

time: 406 us -> 385 us (0.948)
  blocking collectives: 22.7 us -> 0 us
  waiting for transfers between devices: 339 us -> 323 us
  starting transfers between devices: 0.16 us -> 10.6 us
  local copies, waits for them, and re-layouts: 2.69 us -> 9.34 us
    all_gather x1 -> x0, waiting for transfers between devices: 202 us -> none  [on_device(): lax.all_gather(joined, 'fs', axis=0, tiled=True)]
    all_to_all x0 -> x2, waiting for transfers between devices: none -> 103 us  [the longest x1 85.1 us: on_device(): lax.all_to_all(jnp.stack([joined] * lax.axis_size('fs')), 'fs', 0, 0)]
    all_gather x1, waiting for transfers between devices: 85.7 us -> 168 us  [on_device(): down_full = lax.all_gather(down_weight, 'fs', axis=1, tiled=True)]
    all_to_all x1 -> x0, blocking collectives: 22.7 us -> none  [on_device(): lax.all_to_all(hidden_first, 'tp', split_axis=1, concat_axis=0, tiled=True)]
    all_to_all x0 -> x2, starting transfers between devices: none -> 10.5 us  [the longest x1 6.15 us: on_device(): lax.all_to_all(jnp.stack([joined] * lax.axis_size('fs')), 'fs', 0, 0)]
    another operation x0 -> x1, local copies, waits for them, and re-layouts: none -> 4.95 us  [on_device(): jnp.stack([joined] * lax.axis_size('fs'))]
  transfers between devices with their start and end apart: 4 -> 5, of which waited for: 4 -> 5; matrix products, arithmetic and copies ran while one was open for 1% -> 6% of each run, Pallas kernels for 0% -> 0%
where the time goes in v1:
time: 385 us; the launch traced here: 384 us
  waiting for transfers between devices  323 us (84%)
  matrix products  17.4 us (5%)
  between operations  13.8 us (4%)
  starting transfers between devices  10.6 us (3%)
  other arithmetic  9.61 us (2%)
  local copies, waits for them, and re-layouts  9.34 us (2%)
    all_gather x1, waiting for transfers between devices, on_device(): down_full = lax.all_gather(down_weight, 'fs', axis=1, tiled=True)  168 us
    all_to_all x1, waiting for transfers between devices, on_device(): lax.all_to_all(jnp.stack([joined] * lax.axis_size('fs')), 'fs', 0, 0)  85.1 us
    reduce_scatter x1, waiting for transfers between devices, on_device(): lax.psum_scatter(jnp.dot(spread, down_full, preferred_element_type=jnp.fl...  29.6 us
    all_gather x1, waiting for transfers between devices, on_device(): gathered = lax.all_gather(mixed_state, 'tp', axis=0, tiled=True)  22.7 us
    all_to_all x1, waiting for transfers between devices, on_device(): lax.all_to_all(hidden_first, 'tp', split_axis=1, concat_axis=0, tiled=True)  17.4 us
    dot_general x1, matrix products, on_device(): jnp.dot(gathered, jnp.concatenate(lax.all_to_all(jnp.stack([joined] * lax...  10.1 us
  transfers between devices with their start and end apart: 5, of which 5 were waited for; matrix products, arithmetic and copies ran while one was open for 6% of the time, Pallas kernels for 0%

profile of v1, /device:TPU:0, one launch (start us, length us, event | category | flops | bytes accessed | tf_op | source)
XLA Modules:
  0.0 384.2 jit_solution(12662064610168555700)
XLA Ops:
  7.2 0.0 all-gather.3.cloned.1.call-start
  7.2 0.7 all-gather.3.cloned.1.call-update
  7.9 2.5 copy.10
  10.4 4.3 %all-to-all-start = ((bf16[128,4,1408]{0,2,1:T(8,128)(2,1)}), bf16[128,4,1408]{0,2,1:T(8,128)(2,1)}, u32[]{:S(2)}, u32[]{:S(2)}) async-start(bf16[128,4,1408]{0,2,1:T(8,128)(2,1)} %bitcast), calls=%async_computation | async-start | bytes 2883584 | tf_op jit(solution)/shard_map/all_to_all | solution.py:16
  14.8 2.0 pad_maximum_fusion
  16.8 17.4 %all-to-all-done = bf16[128,4,1408]{0,2,1:T(8,128)(2,1)} async-done(((bf16[128,4,1408]{0,2,1:T(8,128)(2,1)}), bf16[128,4,1408]{0,2,1:T(8,128)(2,1)}, u32[]{:S(2)}, u32[]{:S(2)}) %all-to-all-start) | async-done | bytes 1441824 | tf_op jit(solution)/shard_map/all_to_all | solution.py:16
  34.1 5.0 %stack.2 = bf16[4,512,2816]{2,1,0:T(8,128)(2,1)} broadcast(bf16[512,2816]{1,0:T(8,128)(2,1)S(1)} %pad_maximum_fusion), dimensions={1,2} | broadcast | bytes 14417920 | tf_op jit(solution)/shard_map/stack | solution.py:36
  39.1 6.2 %all-to-all-start.1 = ((bf16[4,512,2816]{2,1,0:T(8,128)(2,1)}), bf16[4,512,2816]{2,1,0:T(8,128)(2,1)}, u32[]{:S(2)}, u32[]{:S(2)}) async-start(bf16[4,512,2816]{2,1,0:T(8,128)(2,1)} %stack.2), calls=%async_computation.2 | async-start | bytes 23068672 | tf_op jit(solution)/shard_map/all_to_all | solution.py:36
  45.3 0.0 reduce-scatter.2.cloned.1.call-start
  45.3 1.8 copy.11
  47.1 167.9 %all-gather.3.cloned.1.call-done = bf16[1408,2048]{1,0:T(8,128)(2,1)} async-done(((bf16[1408,512]{1,0:T(8,128)(2,1)}), bf16[1408,2048]{1,0:T(8,128)(2,1)}) %all-gather.3.cloned.1.call-update) | async-done | bytes 5767184 | tf_op jit(solution)/shard_map/all_gather | solution.py:17
  215.0 0.0 copy-start.2
  215.0 0.0 copy-start.3
  215.0 0.0 copy-start
  215.0 7.3 %convolution_convert_fusion = bf16[512,2048]{1,0:T(8,128)(2,1)} fusion(bf16[512,1408]{1,0:T(8,128)(2,1)S(1)} %bitcast.12, bf16[1408,2048]{1,0:T(8,128)(2,1)} %all-gather.3.cloned.1.call-done), kind=kOutput, calls=%fused_computation | convolution fusion | flops 2953838592 | bytes 9306112 | tf_op jit(solution)/shard_map/dot_general | solution.py:19
  222.3 0.0 copy-start.1
  222.3 0.0 reduce-scatter.2.cloned.1.call-update
  222.3 0.0 all-gather.5.cloned.1.call-start
  222.4 0.0 copy-done.2
  222.4 0.0 copy-done.3
  222.4 29.6 %reduce-scatter.2.cloned.1.call-done = bf16[128,2048]{1,0:T(8,128)(2,1)} async-done(((bf16[512,2048]{1,0:T(8,128)(2,1)}), bf16[128,2048]{1,0:T(8,128)(2,1)}) %reduce-scatter.2.cloned.1.call-update) | async-done | bytes 524304 | tf_op jit(solution)/shard_map/reduce_scatter | solution.py:18
  252.0 0.0 copy-done
  252.0 1.3 fusion.1
  253.4 1.4 multiply_reduce_fusion.1
  254.8 0.0 copy-done.1
  254.8 1.6 fusion.2
  256.4 0.3 multiply_reduce_fusion
  256.7 1.1 add_convert_fusion
  257.7 0.0 all-gather.5.cloned.1.call-update
  257.7 22.7 %all-gather.5.cloned.1.call-done = bf16[512,2048]{1,0:T(8,128)(2,1)} async-done(((bf16[128,2048]{1,0:T(8,128)(2,1)}), bf16[512,2048]{1,0:T(8,128)(2,1)}) %all-gather.5.cloned.1.call-update) | async-done | bytes 2097168 | tf_op jit(solution)/shard_map/all_gather | solution.py:30
  280.4 85.1 %all-to-all-done.1 = bf16[4,512,2816]{2,1,0:T(8,128)(2,1)} async-done(((bf16[4,512,2816]{2,1,0:T(8,128)(2,1)}), bf16[4,512,2816]{2,1,0:T(8,128)(2,1)}, u32[]{:S(2)}, u32[]{:S(2)}) %all-to-all-start.1) | async-done | bytes 11534368 | tf_op jit(solution)/shard_map/all_to_all | solution.py:36
  365.6 10.1 %fusion.5 = f32[512,2816]{1,0:T(8,128)S(1)} fusion(bf16[512,2048]{1,0:T(8,128)(2,1)} %all-gather.5.cloned.1.call-done, bf16[2048,2816]{1,0:T(8,128)(2,1)} %bitcast.7), kind=kOutput, calls=%fused_computation.17 | convolution fusion | flops 5905580032 | bytes 19398656 | tf_op jit(solution)/shard_map/dot_general | solution.py:33
  375.7 2.0 fusion
  (6 shorter events, 0.1 us)
Async XLA Ops:
  7.2 207.8 %all-gather.3.cloned.1.call-start = ((), (), s32[]{:S(2)}) async-start(), calls=%async_computation.3 | async-start | bytes 7208960 | tf_op jit(solution)/shard_map/all_gather | solution.py:17
  10.4 23.7 %all-to-all-start = ((bf16[128,4,1408]{0,2,1:T(8,128)(2,1)}), bf16[128,4,1408]{0,2,1:T(8,128)(2,1)}, u32[]{:S(2)}, u32[]{:S(2)}) async-start(bf16[128,4,1408]{0,2,1:T(8,128)(2,1)} %bitcast), calls=%async_computation | async-start | bytes 2883584 | tf_op jit(solution)/shard_map/all_to_all | solution.py:16
  39.1 326.5 %all-to-all-start.1 = ((bf16[4,512,2816]{2,1,0:T(8,128)(2,1)}), bf16[4,512,2816]{2,1,0:T(8,128)(2,1)}, u32[]{:S(2)}, u32[]{:S(2)}) async-start(bf16[4,512,2816]{2,1,0:T(8,128)(2,1)} %stack.2), calls=%async_computation.2 | async-start | bytes 23068672 | tf_op jit(solution)/shard_map/all_to_all | solution.py:36
  45.3 206.8 %reduce-scatter.2.cloned.1.call-start = ((), (), s32[]{:S(2)}) async-start(), calls=%async_computation.4 | async-start | bytes 2621440 | tf_op jit(solution)/shard_map/reduce_scatter | solution.py:18
  215.0 7.3 %copy-start.2 = (f32[2,2048]{1,0:T(2,128)S(1)}, f32[2,2048]{1,0:T(2,128)}, u32[]{:S(2)}) copy-start(f32[2,2048]{1,0:T(2,128)} %param.12) | copy-start | bytes 49156
  215.0 7.4 %copy-start.3 = (f32[2,2048]{1,0:T(2,128)S(1)}, f32[2,2048]{1,0:T(2,128)}, u32[]{:S(2)}) copy-start(f32[2,2048]{1,0:T(2,128)} %param.13) | copy-start | bytes 49156
  215.0 37.0 %copy-start = (bf16[128,2048]{1,0:T(8,128)(2,1)S(1)}, bf16[128,2048]{1,0:T(8,128)(2,1)}, u32[]{:S(2)}) copy-start(bf16[128,2048]{1,0:T(8,128)(2,1)} %param.8) | copy-start | bytes 1572868
  222.3 32.5 %copy-start.1 = (bf16[128,2048]{1,0:T(8,128)(2,1)S(1)}, bf16[128,2048]{1,0:T(8,128)(2,1)}, u32[]{:S(2)}) copy-start(bf16[128,2048]{1,0:T(8,128)(2,1)} %param.11) | copy-start | bytes 1572868
  222.3 58.1 %all-gather.5.cloned.1.call-start = ((), (), s32[]{:S(2)}) async-start(), calls=%async_computation.5 | async-start | bytes 2621440 | tf_op jit(solution)/shard_map/all_gather | solution.py:30
Sparse Core Ops, SparseCore 0:
  9.5 205.4 all-gather.2
  222.4 29.5 reduce-scatter.1
  257.9 22.5 all-gather.4
